TPU v7x, 32 devices: a whole 2x2x4 slice. The times are simulated.
32 devices in a mesh: grp: 2 (over x), ep: 8 (over z, y), tp: 2 (over core).
Axes of the slice: x: 2, y: 2, z: 4, core: 2. Of those that a mesh axis runs over, the one named last changes fastest.
Arguments:
- tokens: bfloat16 [1024, 2048], P(('grp', 'ep')), parts along dimension 0, may hold values from -6 to 6
- norm_gain: float32 [2048], replicated, may hold values from 0.1 to 1.9
- groups: int32 [1024], P(('grp', 'ep')), parts along dimension 0, may hold values from 0 to 1, as said below
- picks: int32 [1024, 4], P(('grp', 'ep')), parts along dimension 0, may hold values from 0 to 7, as said below
- gates: float32 [1024, 4], P(('grp', 'ep')), parts along dimension 0, may hold values from 0.1 to 1
- w_gate: bfloat16 [16, 2048, 512], P('ep', None, 'tp'), may hold values from -0.125 to 0.125
- w_up: bfloat16 [16, 2048, 512], P('ep', None, 'tp'), may hold values from -0.125 to 0.125
- w_down: bfloat16 [16, 512, 2048], P('ep', 'tp'), may hold values from -0.25 to 0.25
Outputs:
- mixed: bfloat16 [1024, 2048], P(('grp', 'ep'), 'tp'), parts along dimension 0
There are 2 independent parts, one for each index of `grp`. A program takes and returns all parts, laid end to end along the dimension named above; an argument that names none is the same for every part. Nothing has to cross between parts.
Inputs may be any that keep to these rules, and one draw needn't show every extreme that they name: `groups`: among the tokens of one device, exactly 32 lie in one common group and all of them name one common expert of it as their first pick; every other token of that device lies in another group. A token's 4 picks are distinct. Among the tokens of one device at most 32 name any one expert (group and pick together), and in every draw one expert is named by exactly 32 tokens of every device.
All inputs are finite; a program needn't handle non-finite values.
Results may differ from a plain program's by a relative error of at most 0.014.
Values may be sent and summed in bfloat16 or wider, within the bound.
No kernel may reach another device: no remote copies, remote signals or barrier semaphores. Data moves between devices by JAX's collectives and lax.ppermute only.
A program may use at most 64 MiB of HBM per device.

v0:
```python
import jax
import jax.numpy as jnp
from jax import lax
from jax.sharding import PartitionSpec as P

GROUPS = 2


epsilon = 1e-06


def run_expert(rows, w_gate, w_up, w_down):
    gate_pre = jnp.einsum("sjiw,jwf->sjif", rows, w_gate, preferred_element_type=jnp.float32)
    up_pre = jnp.einsum("sjiw,jwf->sjif", rows, w_up, preferred_element_type=jnp.float32)
    hidden = (jax.nn.silu(gate_pre) * up_pre).astype(jnp.bfloat16)
    partial_sum = jnp.einsum(
        "sjif,jfw->sjiw", hidden, w_down, preferred_element_type=jnp.float32
    ).astype(jnp.bfloat16)
    return (
        lax.psum_scatter(partial_sum, "tp", scatter_dimension=3, tiled=True)
        .astype(jnp.float32)
        .astype(jnp.bfloat16)
    )


def on_device(tokens, norm_gain, groups, picks, gates, w_gate, w_up, w_down):
    tok_rows, width = tokens.shape
    top = picks.shape[1]
    local = w_gate.shape[0]
    senders = lax.axis_size("ep")
    experts = senders * local
    group_experts = experts // GROUPS
    capacity = tok_rows * top // group_experts
    values = tokens.astype(jnp.float32)
    normed = (
        values * lax.rsqrt(jnp.mean(values * values, axis=-1, keepdims=True) + epsilon) * norm_gain
    ).astype(jnp.bfloat16)
    expert_id = groups[:, None] * group_experts + picks
    count = tok_rows * top
    flat_ids = expert_id.reshape(count)
    onehot = (flat_ids[:, None] == jnp.arange(experts, dtype=jnp.int32)[None, :]).astype(jnp.int32)
    before = jnp.cumsum(onehot, axis=0) - onehot
    target = flat_ids * capacity + jnp.sum(before * onehot, axis=1)
    place = (target[:, None] == jnp.arange(experts * capacity, dtype=jnp.int32)[None, :]).astype(
        jnp.float32
    )
    owner = (
        (jnp.arange(count, dtype=jnp.int32) // top)[:, None]
        == jnp.arange(tok_rows, dtype=jnp.int32)[None, :]
    ).astype(jnp.float32)
    spread = jnp.dot(place.T, owner, precision=lax.Precision.HIGHEST).astype(jnp.bfloat16)
    buffer = jnp.dot(spread, normed, preferred_element_type=jnp.float32).astype(jnp.bfloat16)
    buffer = buffer.reshape(senders, local, capacity, width)
    half = width // lax.axis_size("tp")
    buffer = lax.dynamic_slice_in_dim(buffer, lax.axis_index("tp") * half, half, 3)
    received = lax.all_to_all(buffer, "ep", split_axis=0, concat_axis=0, tiled=True)
    received = lax.all_gather(received, "tp", axis=3, tiled=True)
    result = run_expert(received, w_gate, w_up, w_down)
    returned = lax.all_to_all(result, "ep", split_axis=0, concat_axis=0, tiled=True)
    weighted = place * gates.reshape(count)[:, None]
    combine = jnp.dot(owner.T, weighted, precision=lax.Precision.HIGHEST)
    flat_out = returned.reshape(experts * capacity, returned.shape[3]).astype(jnp.float32)
    mixed = jnp.dot(combine, flat_out, precision=lax.Precision.HIGHEST).astype(jnp.bfloat16)
    return mixed


def solution(mesh):
    in_specs = (
        P(("grp", "ep"), None),
        P(),
        P(("grp", "ep")),
        P(("grp", "ep"), None),
        P(("grp", "ep"), None),
        P("ep", None, "tp"),
        P("ep", None, "tp"),
        P("ep", "tp", None),
    )
    out_specs = P(("grp", "ep"), "tp")
    return jax.shard_map(
        on_device, mesh=mesh, in_specs=in_specs, out_specs=out_specs, check_vma=False
    )
```

profile of v0, /device:TPU:0, one launch (start us, length us, event | category | flops | bytes accessed | tf_op | source)
XLA Modules:
  0.0 117.6 jit_solution(4981290462030990361)
XLA Ops:
  6.5 0.0 copy-start
  6.5 0.0 all-gather.2.cloned.1.call-start
  6.5 0.8 broadcast_multiply_fusion
  7.3 0.7 broadcast_add_fusion
  8.0 0.1 copy.16
  8.1 0.1 eq.61
  8.2 0.1 reshape.59
  8.4 0.6 reduce-window.6
  8.9 0.2 slice_reduce_fusion
  9.2 0.1 fusion.42
  9.3 1.1 fusion.20
  10.4 0.3 convolution_convert_fusion.3
  10.7 1.7 %convolution_convert_fusion.1 = bf16[512,2048]{1,0:T(8,128)(2,1)S(1)} fusion(bf16[512,64]{0,1:T(8,128)(2,1)S(1)} %convolution_convert_fusion.3, bf16[64,2048]{1,0:T(8,128)(2,1)} %param.8, f32[2048]{0:T(1024)} %param.9, f32[64]{0:T(128)S(1)} %add_rsqrt_fusion), kind=kOutput, calls=%fused_computation.1 | convolution fusion | flops 135790592 | bytes 2433280 | tf_op jit(solution)/shard_map/dot_general | solution.py:52
  12.4 0.1 constant_dynamic-slice_fusion
  12.5 32.9 %all_to_all.10 = bf16[8,2,32,1024]{3,2,1,0:T(8,128)(2,1)S(1)} all-to-all(bf16[8,2,32,1024]{3,2,1,0:T(8,128)(2,1)S(1)} %constant_dynamic-slice_fusion), channel_id=1, replica_groups=mesh['grp'=2,'ep'=8,'tp'=2] {'ep'}, dimensions={0} | all-to-all | bytes 2097152 | tf_op jit(solution)/shard_map/all_to_all | solution.py:56
  45.4 1.1 copy.20
  46.5 0.0 all-gather.2.cloned.1.call-update
  46.5 0.0 reduce-scatter.2.cloned.1.call-start
  46.6 9.7 %all-gather.2.cloned.1.call-done = bf16[8,2,32,2048]{3,2,0,1:T(8,128)(2,1)} async-done(((bf16[8,2,32,1024]{3,2,0,1:T(8,128)(2,1)}), bf16[8,2,32,2048]{3,2,0,1:T(8,128)(2,1)}) %all-gather.2.cloned.1.call-update) | async-done | bytes 2097168 | tf_op jit(solution)/shard_map/all_gather | solution.py:57
  56.3 2.9 %fusion.6 = f32[8,2,32,256]{3,2,0,1:T(8,128)S(1)} fusion(bf16[8,2,32,2048]{3,2,0,1:T(8,128)(2,1)} %all-gather.2.cloned.1.call-done, bf16[2,2048,256]{2,1,0:T(8,128)(2,1)} %param.13), kind=kOutput, calls=%fused_computation.8 | convolution fusion | flops 536870912 | bytes 4718592 | tf_op jit(solution)/shard_map/sjiw,jwf->sjif/dot_general | solution.py:13
  59.2 0.0 copy-done
  59.2 4.9 %fusion = bf16[8,2,32,2048]{3,2,0,1:T(8,128)(2,1)} fusion(bf16[2,256,2048]{2,1,0:T(8,128)(2,1)S(1)} %copy-done, bf16[8,2,32,2048]{3,2,0,1:T(8,128)(2,1)} %all-gather.2.cloned.1.call-done, bf16[2,2048,256]{2,1,0:T(8,128)(2,1)} %param.14, f32[8,2,32,256]{3,2,0,1:T(8,128)S(1)} %fusion.6), kind=kOutput, calls=%fused_computation.2 | convolution fusion | flops 1075576832 | bytes 8912896 | tf_op jit(solution)/shard_map/sjif,jfw->sjiw/dot_general | solution.py:16
  64.1 0.0 reduce-scatter.2.cloned.1.call-update
  64.1 0.0 copy-start.1
  64.1 10.9 %reduce-scatter.2.cloned.1.call-done = bf16[8,2,32,1024]{3,2,0,1:T(8,128)(2,1)} async-done(((bf16[8,2,32,2048]{3,2,0,1:T(8,128)(2,1)}), bf16[8,2,32,1024]{3,2,0,1:T(8,128)(2,1)}) %reduce-scatter.2.cloned.1.call-update) | async-done | bytes 1048592 | tf_op jit(solution)/shard_map/reduce_scatter | solution.py:20
  75.1 2.4 %copy.21 = bf16[8,2,32,1024]{3,2,1,0:T(8,128)(2,1)} copy(bf16[8,2,32,1024]{3,2,0,1:T(8,128)(2,1)} %reduce-scatter.2.cloned.1.call-done) | data formatting | bytes 2097152 | tf_op jit(solution)/shard_map/reduce_scatter | solution.py:20
  77.4 5.9 %all-to-all-start.1 = ((bf16[8,2,32,1024]{3,2,1,0:T(8,128)(2,1)}), bf16[8,2,32,1024]{3,2,1,0:T(8,128)(2,1)S(1)}, u32[]{:S(2)}, u32[]{:S(2)}) async-start(bf16[8,2,32,1024]{3,2,1,0:T(8,128)(2,1)} %copy.21), calls=%async_computation.2 | async-start | bytes 2097152 | tf_op jit(solution)/shard_map/all_to_all | solution.py:59
  83.3 0.0 copy-done.1
  83.3 0.1 copy.19
  83.4 0.1 mul.64
  83.5 0.4 fusion.28
  84.0 25.4 %all-to-all-done.1 = bf16[8,2,32,1024]{3,2,1,0:T(8,128)(2,1)S(1)} async-done(((bf16[8,2,32,1024]{3,2,1,0:T(8,128)(2,1)}), bf16[8,2,32,1024]{3,2,1,0:T(8,128)(2,1)S(1)}, u32[]{:S(2)}, u32[]{:S(2)}) %all-to-all-start.1) | async-done | bytes 1048608 | tf_op jit(solution)/shard_map/all_to_all | solution.py:59
  109.4 1.3 %convolution_convert_fusion.2 = bf16[64,1024]{1,0:T(8,128)(2,1)} fusion(f32[64,512]{1,0:T(8,128)S(1)} %fusion.28, bf16[512,1024]{1,0:T(8,128)(2,1)S(1)} %bitcast.64), kind=kOutput, calls=%fused_computation.12 | convolution fusion | flops 402718720 | bytes 1310720 | tf_op jit(solution)/shard_map/dot_general | solution.py:63
  (5 shorter events, 0.1 us)
Async XLA Ops:
  6.5 52.7 %copy-start = (bf16[2,256,2048]{2,1,0:T(8,128)(2,1)S(1)}, bf16[2,256,2048]{2,1,0:T(8,128)(2,1)}, u32[]{:S(2)}) copy-start(bf16[2,256,2048]{2,1,0:T(8,128)(2,1)} %param.15) | copy-start | bytes 6291460
  6.5 49.7 %all-gather.2.cloned.1.call-start = ((), (), s32[]{:S(2)}) async-start(), calls=%async_computation.3 | async-start | bytes 3145728 | tf_op jit(solution)/shard_map/all_gather | solution.py:57
  46.5 28.6 %reduce-scatter.2.cloned.1.call-start = ((), (), s32[]{:S(2)}) async-start(), calls=%async_computation.4 | async-start | bytes 3145728 | tf_op jit(solution)/shard_map/reduce_scatter | solution.py:20
  64.1 19.2 %copy-start.1 = (f32[64,4]{0,1:T(4,128)S(1)}, f32[64,4]{0,1:T(4,128)}, u32[]{:S(2)}) copy-start(f32[64,4]{0,1:T(4,128)} %param.12) | copy-start | bytes 3076
  77.4 32.0 %all-to-all-start.1 = ((bf16[8,2,32,1024]{3,2,1,0:T(8,128)(2,1)}), bf16[8,2,32,1024]{3,2,1,0:T(8,128)(2,1)S(1)}, u32[]{:S(2)}, u32[]{:S(2)}) async-start(bf16[8,2,32,1024]{3,2,1,0:T(8,128)(2,1)} %copy.21), calls=%async_computation.2 | async-start | bytes 2097152 | tf_op jit(solution)/shard_map/all_to_all | solution.py:59
Sparse Core Ops, SparseCore 0:
  46.6 9.5 all-gather.1
  64.3 10.7 reduce-scatter.1
where the time goes:
time: 118 us
  waiting for transfers between devices  46.1 us (39%)
  blocking collectives  32.9 us (28%)
  between operations  13.5 us (11%)
  matrix products  11.6 us (10%)
  starting transfers between devices  5.93 us (5%)
  local copies, waits for them, and re-layouts  4.23 us (4%)
  other arithmetic  3.33 us (3%)
    all_to_all x1, blocking collectives, on_device(): lax.all_to_all(buffer, 'ep', split_axis=0, concat_axis=0, tiled=True)  32.9 us
    all_to_all x1, waiting for transfers between devices, on_device(): lax.all_to_all(result, 'ep', split_axis=0, concat_axis=0, tiled=True)  25.4 us
    reduce_scatter x1, waiting for transfers between devices, run_expert(): lax.psum_scatter(partial_sum, 'tp', scatter_dimension=3, tiled=True)  10.9 us
    all_gather x1, waiting for transfers between devices, on_device(): received = lax.all_gather(received, 'tp', axis=3, tiled=True)  9.71 us
    all_to_all x1, starting transfers between devices, on_device(): lax.all_to_all(result, 'ep', split_axis=0, concat_axis=0, tiled=True)  5.89 us
    dot_general x1, matrix products, run_expert(): jnp.einsum('sjif,jfw->sjiw', hidden, w_down, preferred_element_type=jnp.f...  4.88 us
    dot_general x1, matrix products, run_expert(): jnp.einsum('sjiw,jwf->sjif', rows, w_gate, preferred_element_type=jnp.flo...  2.93 us
  transfers between devices with their start and end apart: 3, of which 3 were waited for; matrix products, arithmetic and copies ran while one was open for 1% of the time, Pallas kernels for 0%

commit v1 on v0

v1 whole, which is shorter than its diff:
```python
import jax
import jax.numpy as jnp
from jax import lax
from jax.experimental import pallas as pl
from jax.sharding import PartitionSpec as P


GROUPS = 2
LANES = 128
SUBLANES = 8

epsilon = 1e-06


def on_device(tokens, norm_gain, groups, picks, gates, w_gate, w_up, w_down):
    tok_rows, width = tokens.shape
    top = picks.shape[1]
    local = w_gate.shape[0]
    senders = lax.axis_size("ep")
    cores = lax.axis_size("tp")
    group_experts = senders * local // GROUPS
    capacity = tok_rows * top // group_experts
    rows = max(capacity, tok_rows - capacity)
    team = senders // GROUPS
    half = width // cores
    ep, tp = lax.axis_index("ep"), lax.axis_index("tp")
    mirror = senders // GROUPS * (GROUPS - 1)

    def across(x, shift):
        return lax.ppermute(x, "ep", [(i, i ^ shift) for i in range(senders)])

    def swap(x):
        return lax.ppermute(x, "tp", [(i, cores - 1 - i) for i in range(cores)])

    near, far, place = pack(
        tokens, norm_gain, groups, picks, gates, rows, team, half, group_experts
    )
    shifts = range(team - 1, 0, -1)

    def gates_of(piece):
        pair = piece[:, half : half + 2 * group_experts].astype(jnp.float32)
        return pair[:, :group_experts] + pair[:, group_experts:]

    got = across(far, mirror)
    last_got = lax.optimization_barrier(gates_of(got))
    last_near = gates_of(near)
    near = [across(near, s) for s in shifts] + [near]
    got = [across(got, s) for s in shifts] + [got]

    def expert_rows(pieces, last):
        own = jnp.concatenate(pieces, axis=0)
        weights = jnp.concatenate([gates_of(piece) for piece in pieces[:-1]] + [last], axis=0)
        weights = lax.dynamic_slice_in_dim(weights, (ep % team) * local, local, 1)
        own = own[:, :half]
        other = swap(own)
        x = jnp.concatenate(
            [jnp.where(tp == 0, own, other), jnp.where(tp == 0, other, own)], axis=1
        )
        return x, weights

    def run_experts(x, weights):
        hidden = []
        for j in range(local):
            g = jnp.dot(x, w_gate[j], preferred_element_type=jnp.float32)
            u = jnp.dot(x, w_up[j], preferred_element_type=jnp.float32)
            hidden.append((jax.nn.silu(g) * u * weights[:, j : j + 1]).astype(jnp.bfloat16))
        hidden = jnp.concatenate(hidden, axis=1)
        y = jnp.dot(
            hidden, w_down.reshape(hidden.shape[1], width), preferred_element_type=jnp.float32
        )
        low, high = y[:, :half], y[:, half:]
        keep = jnp.where(tp == 0, low, high)
        send = jnp.where(tp == 0, high, low).astype(jnp.bfloat16)
        return (keep + swap(send).astype(jnp.float32)).astype(jnp.bfloat16)

    def collect(part):
        pieces = [part[i * rows : (i + 1) * rows] for i in range(team)]
        total = pieces[-1].astype(jnp.float32)
        for piece, s in zip(pieces, shifts):
            total = total + across(piece, s).astype(jnp.float32)
        return total.astype(jnp.bfloat16)

    near_part = run_experts(*expert_rows(near, last_near))
    got_part = run_experts(*expert_rows(got, last_got))
    far = across(collect(got_part), mirror)
    near = collect(near_part)
    out = lax.dot_general(
        place,
        jnp.concatenate([near, far], axis=0),
        (((0,), (0,)), ((), ())),
        preferred_element_type=jnp.float32,
    )
    return out.astype(jnp.bfloat16)


def pack(tokens, norm_gain, groups, picks, gates, rows, team, half, group_experts):
    tok_rows, width = tokens.shape
    top = picks.shape[1]
    pad = -(-2 * group_experts // LANES) * LANES

    def kernel(tok_ref, gain_ref, group_ref, picks_ref, gates_ref, near_ref, far_ref, place_ref):
        my_group = lax.axis_index("ep") // team
        at = pl.multiple_of(lax.axis_index("tp") * half, LANES)
        values = tok_ref[...].astype(jnp.float32)
        scale = lax.rsqrt(jnp.mean(values * values, axis=-1, keepdims=True) + epsilon)
        mine = tok_ref[:, pl.ds(at, half)].astype(jnp.float32)
        normed = (mine * scale * gain_ref[:, pl.ds(at, half)]).astype(jnp.bfloat16)
        row = lax.broadcasted_iota(jnp.int32, (pad, tok_rows), 0)
        expert = jnp.where(row < group_experts, row, row - group_experts)
        table = jnp.zeros((pad, tok_rows), jnp.float32)
        for k in range(top):
            table += jnp.where(picks_ref[k : k + 1] == expert, gates_ref[k : k + 1], 0.0)
        high = table.astype(jnp.bfloat16).astype(jnp.float32)
        table = jnp.where(row < group_experts, high, table - high).astype(jnp.bfloat16)
        group = lax.broadcasted_iota(jnp.int32, (SUBLANES, tok_rows), 0)
        member = jnp.where(group_ref[...] == group, 1.0, 0.0)
        earlier = lax.broadcasted_iota(jnp.int32, (tok_rows, tok_rows), 0)
        later = lax.broadcasted_iota(jnp.int32, (tok_rows, tok_rows), 1)
        before = jnp.where(earlier < later, 1.0, 0.0).astype(jnp.bfloat16)
        ahead = jnp.dot(member.astype(jnp.bfloat16), before, preferred_element_type=jnp.float32)
        position = jnp.sum(member * ahead, axis=0, keepdims=True).astype(jnp.int32)
        target = jnp.where(group_ref[...] == my_group, 0, rows) + position
        slot = lax.broadcasted_iota(jnp.int32, (GROUPS * rows, tok_rows), 0)
        place = jnp.where(slot == target, 1.0, 0.0).astype(jnp.bfloat16)
        place_ref[...] = place
        packed = jnp.dot(place, normed, preferred_element_type=jnp.float32).astype(jnp.bfloat16)
        near_ref[:, :half] = packed[:rows]
        far_ref[:, :half] = packed[rows:]
        packed = lax.dot_general(
            place, table, (((1,), (1,)), ((), ())), preferred_element_type=jnp.float32
        ).astype(jnp.bfloat16)
        near_ref[:, half:] = packed[:rows]
        far_ref[:, half:] = packed[rows:]

    block = jax.ShapeDtypeStruct((rows, half + pad), jnp.bfloat16)
    return pl.pallas_call(
        kernel,
        out_shape=(block, block, jax.ShapeDtypeStruct((GROUPS * rows, tok_rows), jnp.bfloat16)),
    )(
        tokens,
        norm_gain.reshape(1, width),
        groups.reshape(1, tok_rows),
        picks.T,
        gates.T,
    )


def solution(mesh):
    in_specs = (
        P(("grp", "ep"), None),
        P(),
        P(("grp", "ep")),
        P(("grp", "ep"), None),
        P(("grp", "ep"), None),
        P("ep", None, "tp"),
        P("ep", None, "tp"),
        P("ep", "tp", None),
    )
    out_specs = P(("grp", "ep"), "tp")
    return jax.shard_map(
        on_device, mesh=mesh, in_specs=in_specs, out_specs=out_specs, check_vma=False
    )
```

time: 118 us -> 45.5 us (0.39)
  waiting for transfers between devices: 46.1 us -> 11.4 us
  blocking collectives: 32.9 us -> 0 us
  starting transfers between devices: 5.93 us -> 22.2 us
  between operations: 13.5 us -> 0.25 us
  matrix products: 11.6 us -> 5.64 us
  local copies, waits for them, and re-layouts: 4.23 us -> 0.88 us
  Pallas kernels: 0 us -> 2.12 us
    all_to_all x1 -> x0, blocking collectives: 32.9 us -> none  [on_device(): lax.all_to_all(buffer, 'ep', split_axis=0, concat_axis=0, tiled=True)]
    all_to_all x1 -> x0, waiting for transfers between devices: 25.4 us -> none  [on_device(): lax.all_to_all(result, 'ep', split_axis=0, concat_axis=0, tiled=True)]
    ppermute x0 -> x18, starting transfers between devices: none -> 22.2 us  [the longest x14 21.4 us: across(): return lax.ppermute(x, 'ep', [(i, i ^ shift) for i in range(senders)])]
    ppermute x0 -> x18, waiting for transfers between devices: none -> 11.4 us  [the longest x14 10.3 us: across(): return lax.ppermute(x, 'ep', [(i, i ^ shift) for i in range(senders)])]
    reduce_scatter x1 -> x0, waiting for transfers between devices: 10.9 us -> none  [run_expert(): lax.psum_scatter(partial_sum, 'tp', scatter_dimension=3, tiled=True)]
    all_gather x1 -> x0, waiting for transfers between devices: 9.71 us -> none  [on_device(): received = lax.all_gather(received, 'tp', axis=3, tiled=True)]
    dot_general x6 -> x11, matrix products: 11.6 us -> 5.64 us  [the longest x4 2.62 us: run_experts(): g = jnp.dot(x, w_gate[j], preferred_element_type=jnp.float32)]
    all_to_all x1 -> x0, starting transfers between devices: 5.89 us -> none  [on_device(): lax.all_to_all(result, 'ep', split_axis=0, concat_axis=0, tiled=True)]
  transfers between devices with their start and end apart: 3 -> 18, of which waited for: 3 -> 8; matrix products, arithmetic and copies ran while one was open for 1% -> 16% of each run, Pallas kernels for 0% -> 0%
where the time goes in v1:
time: 45.5 us; the launch traced here: 45.3 us
  starting transfers between devices  22.2 us (49%)
  waiting for transfers between devices  11.4 us (25%)
  matrix products  5.64 us (12%)
  other arithmetic  2.84 us (6%)
  Pallas kernels  2.12 us (5%)
  local copies, waits for them, and re-layouts  0.88 us (2%)
    ppermute x14, starting transfers between devices, across(): return lax.ppermute(x, 'ep', [(i, i ^ shift) for i in range(senders)])  21.4 us
    ppermute x14, waiting for transfers between devices, across(): return lax.ppermute(x, 'ep', [(i, i ^ shift) for i in range(senders)])  10.3 us
    dot_general x4, matrix products, run_experts(): g = jnp.dot(x, w_gate[j], preferred_element_type=jnp.float32)  2.62 us
    pallas_call x1, Pallas kernels, pack(): pl.pallas_call(kernel, out_shape=(block, block, jax.ShapeDtypeStruct((GRO...  2.12 us
    dot_general x4, matrix products, run_experts(): u = jnp.dot(x, w_up[j], preferred_element_type=jnp.float32)  1.24 us
    ppermute x4, waiting for transfers between devices, swap(): return lax.ppermute(x, 'tp', [(i, cores - 1 - i) for i in range(cores)])  1.12 us
  transfers between devices with their start and end apart: 18, of which 8 were waited for; matrix products, arithmetic and copies ran while one was open for 16% of the time, Pallas kernels for 0%

profile of v1, /device:TPU:0, one launch (start us, length us, event | category | flops | bytes accessed | tf_op | source)
XLA Modules:
  0.0 45.3 jit_solution(5010872655494658981)
XLA Ops:
  0.0 2.1 %shard_map.82 = (bf16[32,1152]{1,0:T(8,128)(2,1)}, bf16[32,1152]{1,0:T(8,128)(2,1)}, bf16[64,64]{1,0:T(8,128)(2,1)}) custom-call(bf16[64,2048]{1,0:T(8,128)(2,1)} %tok_ref.1, f32[1,2048]{1,0:T(1,128)} %bitcast.46, s32[1,64]{1,0:T(1,128)} %bitcast.49, s32[4,64]{1,0:T(4,128)} %bitcast.47, f32[4,64]{1,0:T(4,128)} %bitcast.48), custom_call_target="tpu_custom_call" | custom-call | tf_op jit(solution)/shard_map/pallas_call | solution.py:136
  2.1 3.0 %collective-permute-start.2 = (bf16[32,1152]{1,0:T(8,128)(2,1)}, bf16[32,1152]{1,0:T(8,128)(2,1)S(1)}, u32[]{:S(2)}, u32[]{:S(2)}) collective-permute-start(bf16[32,1152]{1,0:T(8,128)(2,1)} %get-tuple-element.9), channel_id=1, source_target_pairs={{0,2},{2,0},{4,6},{6,4},{8,10},{10,8},{12,14},{14,12},{1,3},{3,1},... | collective-permute-start | bytes 221192 | tf_op jit(solution)/shard_map/ppermute | solution.py:30
  5.1 1.6 %collective-permute-start.1 = (bf16[32,1152]{1,0:T(8,128)(2,1)}, bf16[32,1152]{1,0:T(8,128)(2,1)S(1)}, u32[]{:S(2)}, u32[]{:S(2)}) collective-permute-start(bf16[32,1152]{1,0:T(8,128)(2,1)} %get-tuple-element.9), channel_id=1, source_target_pairs={{0,4},{2,6},{4,0},{6,2},{8,12},{10,14},{12,8},{14,10},{1,5},{3,7},... | collective-permute-start | bytes 221192 | tf_op jit(solution)/shard_map/ppermute | solution.py:30
  6.7 3.0 %collective-permute-start.8 = (bf16[32,1152]{1,0:T(8,128)(2,1)}, bf16[32,1152]{1,0:T(8,128)(2,1)S(1)}, u32[]{:S(2)}, u32[]{:S(2)}) collective-permute-start(bf16[32,1152]{1,0:T(8,128)(2,1)} %get-tuple-element.10), channel_id=1, source_target_pairs={{0,8},{2,10},{4,12},{6,14},{8,0},{10,2},{12,4},{14,6},{1,9},{3,11}... | collective-permute-start | bytes 221192 | tf_op jit(solution)/shard_map/ppermute | solution.py:30
  9.7 0.7 %slice_convert_fusion.7 = f32[32,16]{1,0:T(8,128)S(1)} fusion(bf16[32,1152]{1,0:T(8,128)(2,1)} %get-tuple-element.9), kind=kLoop, calls=%fused_computation.73 | loop fusion | flops 512 | bytes 3072 | tf_op jit(solution)/shard_map/convert_element_type | solution.py:41
  10.4 0.1 slice_add_fusion.4
  10.5 0.1 copy.12
  10.5 1.8 %collective-permute-done.8 = bf16[32,1152]{1,0:T(8,128)(2,1)S(1)} collective-permute-done((bf16[32,1152]{1,0:T(8,128)(2,1)}, bf16[32,1152]{1,0:T(8,128)(2,1)S(1)}, u32[]{:S(2)}, u32[]{:S(2)}) %collective-permute-start.8) | collective-permute-done | bytes 73760 | tf_op jit(solution)/shard_map/ppermute | solution.py:30
  12.3 0.1 slice_add_fusion
  12.4 0.0 collective-permute-done.2
  12.4 0.1 slice_add_fusion.5
  12.5 0.1 slice_add_fusion.6
  12.6 0.1 copy.16
  12.6 0.1 copy.11
  12.7 0.1 copy.10
  12.8 0.1 slice_add_fusion.7
  12.9 0.1 copy.9
  12.9 0.9 %pad_maximum_fusion.5 = bf16[128,1024]{1,0:T(8,128)(2,1)S(1)} fusion(bf16[32,1152]{1,0:T(8,128)(2,1)} %get-tuple-element.9, bf16[32,1152]{1,0:T(8,128)(2,1)S(1)} %collective-permute-done.2, bf16[32,1152]{1,0:T(8,128)(2,1)S(1)} %collective-permute-done.1, bf16[32,1152]{1,0:T(8,128)(2,1)S(1)} %collective-permute-done), kind=kLoop, calls=%fused_computation.34 | loop fusion | flops 1048576 | bytes 557056 | tf_op jit(solution)/shard_map/concatenate | solution.py:51
  13.8 0.1 collective-permute-start.3
  13.9 2.4 %collective-permute-start.11 = (bf16[32,1152]{1,0:T(8,128)(2,1)S(1)}, bf16[32,1152]{1,0:T(8,128)(2,1)S(1)}, u32[]{:S(2)}, u32[]{:S(2)}) collective-permute-start(bf16[32,1152]{1,0:T(8,128)(2,1)S(1)} %collective-permute-done.8), channel_id=1, source_target_pairs={{0,2},{2,0},{4,6},{6,4},{8,10},{10,8},{12,14},{14,12},{1,3},{3,1},... | collective-permute-start | bytes 221192 | tf_op jit(solution)/shard_map/ppermute | solution.py:30
  16.3 1.5 %collective-permute-start.10 = (bf16[32,1152]{1,0:T(8,128)(2,1)S(1)}, bf16[32,1152]{1,0:T(8,128)(2,1)S(1)}, u32[]{:S(2)}, u32[]{:S(2)}) collective-permute-start(bf16[32,1152]{1,0:T(8,128)(2,1)S(1)} %collective-permute-done.8), channel_id=1, source_target_pairs={{0,4},{2,6},{4,0},{6,2},{8,12},{10,14},{12,8},{14,10},{1,5},{3,7},... | collective-permute-start | bytes 221192 | tf_op jit(solution)/shard_map/ppermute | solution.py:30
  17.7 0.6 %collective-permute-start.9 = (bf16[32,1152]{1,0:T(8,128)(2,1)S(1)}, bf16[32,1152]{1,0:T(8,128)(2,1)S(1)}, u32[]{:S(2)}, u32[]{:S(2)}) collective-permute-start(bf16[32,1152]{1,0:T(8,128)(2,1)S(1)} %collective-permute-done.8), channel_id=1, source_target_pairs={{0,6},{2,4},{4,2},{6,0},{8,14},{10,12},{12,10},{14,8},{1,7},{3,5},... | collective-permute-start | bytes 221192 | tf_op jit(solution)/shard_map/ppermute | solution.py:30
  18.4 0.1 pad_maximum_fusion.8
  18.4 0.7 %collective-permute-done.11 = bf16[32,1152]{1,0:T(8,128)(2,1)S(1)} collective-permute-done((bf16[32,1152]{1,0:T(8,128)(2,1)S(1)}, bf16[32,1152]{1,0:T(8,128)(2,1)S(1)}, u32[]{:S(2)}, u32[]{:S(2)}) %collective-permute-start.11) | collective-permute-done | bytes 73760 | tf_op jit(solution)/shard_map/ppermute | solution.py:30
  19.1 0.1 slice_add_fusion.1
  19.2 1.4 %collective-permute-done.10 = bf16[32,1152]{1,0:T(8,128)(2,1)S(1)} collective-permute-done((bf16[32,1152]{1,0:T(8,128)(2,1)S(1)}, bf16[32,1152]{1,0:T(8,128)(2,1)S(1)}, u32[]{:S(2)}, u32[]{:S(2)}) %collective-permute-start.10) | collective-permute-done | bytes 73760 | tf_op jit(solution)/shard_map/ppermute | solution.py:30
  20.6 0.1 slice_add_fusion.2
  20.7 0.1 copy.15
  20.8 0.1 copy.14
  20.8 2.2 %collective-permute-done.9 = bf16[32,1152]{1,0:T(8,128)(2,1)S(1)} collective-permute-done((bf16[32,1152]{1,0:T(8,128)(2,1)S(1)}, bf16[32,1152]{1,0:T(8,128)(2,1)S(1)}, u32[]{:S(2)}, u32[]{:S(2)}) %collective-permute-start.9) | collective-permute-done | bytes 73760 | tf_op jit(solution)/shard_map/ppermute | solution.py:30
  23.0 0.1 slice_add_fusion.3
  23.1 0.1 copy.13
  23.1 0.1 pad_maximum_fusion.9
  23.3 0.1 collective-permute-start.12
  23.4 0.0 copy-start.3
  23.4 1.7 %fusion.6 = f32[128,256]{1,0:T(8,128)S(1)} fusion(bf16[2,2048,256]{2,1,0:T(8,128)(2,1)} %param.13, bf16[128,1024]{1,0:T(8,128)(2,1)S(1)} %get-tuple-element.12, bf16[128,1024]{1,0:T(8,128)(2,1)S(1)} %get-tuple-element.11), kind=kOutput, calls=%fused_computation.7 | convolution fusion | flops 135266304 | bytes 1703936 | tf_op jit(solution)/shard_map/dot_general | solution.py:64
  25.1 0.3 fusion.14
  25.5 0.3 copy-done.3
  25.8 0.3 multiply_convert_fusion.2
  26.1 0.3 multiply_convert_fusion.3
  26.4 0.5 %fusion.24 = f32[128,2048]{1,0:T(8,128)S(1)} fusion(bf16[512,2048]{1,0:T(8,128)(2,1)S(1)} %bitcast.44, bf16[128,256]{1,0:T(8,128)(2,1)S(1)} %multiply_convert_fusion.2, bf16[128,256]{1,0:T(8,128)(2,1)S(1)} %multiply_convert_fusion.3), kind=kOutput, calls=%fused_computation.41 | convolution fusion | flops 268697600 | bytes 3276800 | tf_op jit(solution)/shard_map/dot_general | solution.py:68
  26.9 0.1 select_convert_fusion.1
  26.9 0.3 collective-permute-start.4
  27.2 0.3 fusion.4
  27.5 0.3 fusion.12
  27.9 0.3 multiply_convert_fusion
  28.2 0.3 multiply_convert_fusion.1
  28.5 0.5 fusion.28
  29.0 0.1 select_convert_fusion
  29.0 0.4 collective-permute-start.13
  29.4 0.1 add_convert_fusion.1
  29.5 1.1 %collective-permute-done.13 = bf16[128,1024]{1,0:T(8,128)(2,1)S(1)} collective-permute-done((bf16[128,1024]{1,0:T(8,128)(2,1)S(1)}, bf16[128,1024]{1,0:T(8,128)(2,1)S(1)}, u32[]{:S(2)}, u32[]{:S(2)}) %collective-permute-start.13) | collective-permute-done | bytes 262176 | tf_op jit(solution)/shard_map/ppermute | solution.py:33
  30.6 0.1 add_convert_fusion
  30.8 1.6 %collective-permute-start.14 = (bf16[32,1024]{1,0:T(8,128)(2,1)S(1)}, bf16[32,1024]{1,0:T(8,128)(2,1)S(1)}, u32[]{:S(2)}, u32[]{:S(2)}) collective-permute-start(bf16[32,1024]{1,0:T(8,128)(2,1)S(1)} %get-tuple-element.18), channel_id=1, source_target_pairs={{0,6},{2,4},{4,2},{6,0},{8,14},{10,12},{12,10},{14,8},{1,7},{3,5},... | collective-permute-start | bytes 196616 | tf_op jit(solution)/shard_map/ppermute | solution.py:30
  32.4 1.2 %collective-permute-start.16 = (bf16[32,1024]{1,0:T(8,128)(2,1)S(1)}, bf16[32,1024]{1,0:T(8,128)(2,1)S(1)}, u32[]{:S(2)}, u32[]{:S(2)}) collective-permute-start(bf16[32,1024]{1,0:T(8,128)(2,1)S(1)} %get-tuple-element.19), channel_id=1, source_target_pairs={{0,2},{2,0},{4,6},{6,4},{8,10},{10,8},{12,14},{14,12},{1,3},{3,1},... | collective-permute-start | bytes 196616 | tf_op jit(solution)/shard_map/ppermute | solution.py:30
  33.5 0.8 %collective-permute-start.15 = (bf16[32,1024]{1,0:T(8,128)(2,1)S(1)}, bf16[32,1024]{1,0:T(8,128)(2,1)S(1)}, u32[]{:S(2)}, u32[]{:S(2)}) collective-permute-start(bf16[32,1024]{1,0:T(8,128)(2,1)S(1)} %get-tuple-element.20), channel_id=1, source_target_pairs={{0,4},{2,6},{4,0},{6,2},{8,12},{10,14},{12,8},{14,10},{1,5},{3,7},... | collective-permute-start | bytes 196616 | tf_op jit(solution)/shard_map/ppermute | solution.py:30
  34.3 1.6 %collective-permute-start.5 = (bf16[32,1024]{1,0:T(8,128)(2,1)S(1)}, bf16[32,1024]{1,0:T(8,128)(2,1)S(1)}, u32[]{:S(2)}, u32[]{:S(2)}) collective-permute-start(bf16[32,1024]{1,0:T(8,128)(2,1)S(1)} %get-tuple-element.15), channel_id=1, source_target_pairs={{0,6},{2,4},{4,2},{6,0},{8,14},{10,12},{12,10},{14,8},{1,7},{3,5},... | collective-permute-start | bytes 196616 | tf_op jit(solution)/shard_map/ppermute | solution.py:30
  35.9 1.2 %collective-permute-start.7 = (bf16[32,1024]{1,0:T(8,128)(2,1)S(1)}, bf16[32,1024]{1,0:T(8,128)(2,1)S(1)}, u32[]{:S(2)}, u32[]{:S(2)}) collective-permute-start(bf16[32,1024]{1,0:T(8,128)(2,1)S(1)} %get-tuple-element.16), channel_id=1, source_target_pairs={{0,2},{2,0},{4,6},{6,4},{8,10},{10,8},{12,14},{14,12},{1,3},{3,1},... | collective-permute-start | bytes 196616 | tf_op jit(solution)/shard_map/ppermute | solution.py:30
  37.1 0.8 %collective-permute-start.6 = (bf16[32,1024]{1,0:T(8,128)(2,1)S(1)}, bf16[32,1024]{1,0:T(8,128)(2,1)S(1)}, u32[]{:S(2)}, u32[]{:S(2)}) collective-permute-start(bf16[32,1024]{1,0:T(8,128)(2,1)S(1)} %get-tuple-element.17), channel_id=1, source_target_pairs={{0,4},{2,6},{4,0},{6,2},{8,12},{10,14},{12,8},{14,10},{1,5},{3,7},... | collective-permute-start | bytes 196616 | tf_op jit(solution)/shard_map/ppermute | solution.py:30
  37.9 0.6 %collective-permute-done.15 = bf16[32,1024]{1,0:T(8,128)(2,1)S(1)} collective-permute-done((bf16[32,1024]{1,0:T(8,128)(2,1)S(1)}, bf16[32,1024]{1,0:T(8,128)(2,1)S(1)}, u32[]{:S(2)}, u32[]{:S(2)}) %collective-permute-start.15) | collective-permute-done | bytes 65568 | tf_op jit(solution)/shard_map/ppermute | solution.py:30
  38.5 2.3 %collective-permute-start.17 = (bf16[32,1024]{1,0:T(8,128)(2,1)S(1)}, bf16[32,1024]{1,0:T(8,128)(2,1)S(1)}, u32[]{:S(2)}, u32[]{:S(2)}) collective-permute-start(bf16[32,1024]{1,0:T(8,128)(2,1)S(1)} %add_convert_fusion.2), channel_id=1, source_target_pairs={{0,8},{2,10},{4,12},{6,14},{8,0},{10,2},{12,4},{14,6},{1,9},{3,11}... | collective-permute-start | bytes 196616 | tf_op jit(solution)/shard_map/ppermute | solution.py:30
  40.8 1.2 %collective-permute-done.6 = bf16[32,1024]{1,0:T(8,128)(2,1)S(1)} collective-permute-done((bf16[32,1024]{1,0:T(8,128)(2,1)S(1)}, bf16[32,1024]{1,0:T(8,128)(2,1)S(1)}, u32[]{:S(2)}, u32[]{:S(2)}) %collective-permute-start.6) | collective-permute-done | bytes 65568 | tf_op jit(solution)/shard_map/ppermute | solution.py:30
  42.1 2.4 %collective-permute-done.17 = bf16[32,1024]{1,0:T(8,128)(2,1)S(1)} collective-permute-done((bf16[32,1024]{1,0:T(8,128)(2,1)S(1)}, bf16[32,1024]{1,0:T(8,128)(2,1)S(1)}, u32[]{:S(2)}, u32[]{:S(2)}) %collective-permute-start.17) | collective-permute-done | bytes 65568 | tf_op jit(solution)/shard_map/ppermute | solution.py:30
  44.5 0.9 %convolution_convert_fusion = bf16[64,1024]{1,0:T(8,128)(2,1)} fusion(bf16[64,64]{1,0:T(8,128)(2,1)S(1)} %copy-done.1, bf16[32,1024]{1,0:T(8,128)(2,1)S(1)} %collective-permute-done.17, bf16[32,1024]{1,0:T(8,128)(2,1)S(1)} %add_convert_fusion.3), kind=kOutput, calls=%fused_computation | convolution fusion | flops 8716288 | bytes 270336 | tf_op jit(solution)/shard_map/dot_general | solution.py:87
  (33 shorter events, 0.3 us)
Async XLA Ops:
  0.0 26.4 %copy-start = (bf16[2,256,2048]{2,1,0:T(8,128)(2,1)S(1)}, bf16[2,256,2048]{2,1,0:T(8,128)(2,1)}, u32[]{:S(2)}) copy-start(bf16[2,256,2048]{2,1,0:T(8,128)(2,1)} %param.15) | copy-start | bytes 6291460
  2.1 10.3 %collective-permute-start.2 = (bf16[32,1152]{1,0:T(8,128)(2,1)}, bf16[32,1152]{1,0:T(8,128)(2,1)S(1)}, u32[]{:S(2)}, u32[]{:S(2)}) collective-permute-start(bf16[32,1152]{1,0:T(8,128)(2,1)} %get-tuple-element.9), channel_id=1, source_target_pairs={{0,2},{2,0},{4,6},{6,4},{8,10},{10,8},{12,14},{14,12},{1,3},{3,1},... | collective-permute-start | bytes 221192 | tf_op jit(solution)/shard_map/ppermute | solution.py:30
  5.1 7.4 %collective-permute-start.1 = (bf16[32,1152]{1,0:T(8,128)(2,1)}, bf16[32,1152]{1,0:T(8,128)(2,1)S(1)}, u32[]{:S(2)}, u32[]{:S(2)}) collective-permute-start(bf16[32,1152]{1,0:T(8,128)(2,1)} %get-tuple-element.9), channel_id=1, source_target_pairs={{0,4},{2,6},{4,0},{6,2},{8,12},{10,14},{12,8},{14,10},{1,5},{3,7},... | collective-permute-start | bytes 221192 | tf_op jit(solution)/shard_map/ppermute | solution.py:30
  6.7 6.1 %collective-permute-start = (bf16[32,1152]{1,0:T(8,128)(2,1)}, bf16[32,1152]{1,0:T(8,128)(2,1)S(1)}, u32[]{:S(2)}, u32[]{:S(2)}) collective-permute-start(bf16[32,1152]{1,0:T(8,128)(2,1)} %get-tuple-element.9), channel_id=1, source_target_pairs={{0,6},{2,4},{4,2},{6,0},{8,14},{10,12},{12,10},{14,8},{1,7},{3,5},... | collective-permute-start | bytes 221192 | tf_op jit(solution)/shard_map/ppermute | solution.py:30
  6.7 5.6 %collective-permute-start.8 = (bf16[32,1152]{1,0:T(8,128)(2,1)}, bf16[32,1152]{1,0:T(8,128)(2,1)S(1)}, u32[]{:S(2)}, u32[]{:S(2)}) collective-permute-start(bf16[32,1152]{1,0:T(8,128)(2,1)} %get-tuple-element.10), channel_id=1, source_target_pairs={{0,8},{2,10},{4,12},{6,14},{8,0},{10,2},{12,4},{14,6},{1,9},{3,11}... | collective-permute-start | bytes 221192 | tf_op jit(solution)/shard_map/ppermute | solution.py:30
  13.8 9.5 %collective-permute-start.3 = (bf16[128,1024]{1,0:T(8,128)(2,1)S(1)}, bf16[128,1024]{1,0:T(8,128)(2,1)S(1)}, u32[]{:S(2)}, u32[]{:S(2)}) collective-permute-start(bf16[128,1024]{1,0:T(8,128)(2,1)S(1)} %pad_maximum_fusion.5), channel_id=1, source_target_pairs={{0,1},{1,0},{2,3},{3,2},{4,5},{5,4},{6,7},{7,6},{8,9},{9,8},{10,11... | collective-permute-start | bytes 786440 | tf_op jit(solution)/shard_map/ppermute | solution.py:33
  13.9 5.2 %collective-permute-start.11 = (bf16[32,1152]{1,0:T(8,128)(2,1)S(1)}, bf16[32,1152]{1,0:T(8,128)(2,1)S(1)}, u32[]{:S(2)}, u32[]{:S(2)}) collective-permute-start(bf16[32,1152]{1,0:T(8,128)(2,1)S(1)} %collective-permute-done.8), channel_id=1, source_target_pairs={{0,2},{2,0},{4,6},{6,4},{8,10},{10,8},{12,14},{14,12},{1,3},{3,1},... | collective-permute-start | bytes 221192 | tf_op jit(solution)/shard_map/ppermute | solution.py:30
  16.3 4.4 %collective-permute-start.10 = (bf16[32,1152]{1,0:T(8,128)(2,1)S(1)}, bf16[32,1152]{1,0:T(8,128)(2,1)S(1)}, u32[]{:S(2)}, u32[]{:S(2)}) collective-permute-start(bf16[32,1152]{1,0:T(8,128)(2,1)S(1)} %collective-permute-done.8), channel_id=1, source_target_pairs={{0,4},{2,6},{4,0},{6,2},{8,12},{10,14},{12,8},{14,10},{1,5},{3,7},... | collective-permute-start | bytes 221192 | tf_op jit(solution)/shard_map/ppermute | solution.py:30
  17.7 5.3 %collective-permute-start.9 = (bf16[32,1152]{1,0:T(8,128)(2,1)S(1)}, bf16[32,1152]{1,0:T(8,128)(2,1)S(1)}, u32[]{:S(2)}, u32[]{:S(2)}) collective-permute-start(bf16[32,1152]{1,0:T(8,128)(2,1)S(1)} %collective-permute-done.8), channel_id=1, source_target_pairs={{0,6},{2,4},{4,2},{6,0},{8,14},{10,12},{12,10},{14,8},{1,7},{3,5},... | collective-permute-start | bytes 221192 | tf_op jit(solution)/shard_map/ppermute | solution.py:30
  23.1 2.0 %copy-start.2 = (bf16[2,2048,256]{2,1,0:T(8,128)(2,1)S(1)}, bf16[2,2048,256]{2,1,0:T(8,128)(2,1)}, u32[]{:S(2)}) copy-start(bf16[2,2048,256]{2,1,0:T(8,128)(2,1)} %param.13) | copy-start | bytes 6291460
  23.3 3.9 %collective-permute-start.12 = (bf16[128,1024]{1,0:T(8,128)(2,1)S(1)}, bf16[128,1024]{1,0:T(8,128)(2,1)S(1)}, u32[]{:S(2)}, u32[]{:S(2)}) collective-permute-start(bf16[128,1024]{1,0:T(8,128)(2,1)S(1)} %pad_maximum_fusion.2), channel_id=1, source_target_pairs={{0,1},{1,0},{2,3},{3,2},{4,5},{5,4},{6,7},{7,6},{8,9},{9,8},{10,11... | collective-permute-start | bytes 786440 | tf_op jit(solution)/shard_map/ppermute | solution.py:33
  23.4 2.3 %copy-start.3 = (bf16[2,2048,256]{2,1,0:T(8,128)(2,1)S(1)}, bf16[2,2048,256]{2,1,0:T(8,128)(2,1)}, u32[]{:S(2)}) copy-start(bf16[2,2048,256]{2,1,0:T(8,128)(2,1)} %param.14) | copy-start | bytes 6291460
  26.9 2.5 %collective-permute-start.4 = (bf16[128,1024]{1,0:T(8,128)(2,1)S(1)}, bf16[128,1024]{1,0:T(8,128)(2,1)S(1)}, u32[]{:S(2)}, u32[]{:S(2)}) collective-permute-start(bf16[128,1024]{1,0:T(8,128)(2,1)S(1)} %select_convert_fusion.1), channel_id=1, source_target_pairs={{0,1},{1,0},{2,3},{3,2},{4,5},{5,4},{6,7},{7,6},{8,9},{9,8},{10,11... | collective-permute-start | bytes 786440 | tf_op jit(solution)/shard_map/ppermute | solution.py:33
  29.0 15.4 %copy-start.1 = (bf16[64,64]{1,0:T(8,128)(2,1)S(1)}, bf16[64,64]{1,0:T(8,128)(2,1)}, u32[]{:S(2)}) copy-start(bf16[64,64]{1,0:T(8,128)(2,1)} %get-tuple-element.8) | copy-start | bytes 24580
  29.0 1.6 %collective-permute-start.13 = (bf16[128,1024]{1,0:T(8,128)(2,1)S(1)}, bf16[128,1024]{1,0:T(8,128)(2,1)S(1)}, u32[]{:S(2)}, u32[]{:S(2)}) collective-permute-start(bf16[128,1024]{1,0:T(8,128)(2,1)S(1)} %select_convert_fusion), channel_id=1, source_target_pairs={{0,1},{1,0},{2,3},{3,2},{4,5},{5,4},{6,7},{7,6},{8,9},{9,8},{10,11... | collective-permute-start | bytes 786440 | tf_op jit(solution)/shard_map/ppermute | solution.py:33
  30.8 6.4 %collective-permute-start.14 = (bf16[32,1024]{1,0:T(8,128)(2,1)S(1)}, bf16[32,1024]{1,0:T(8,128)(2,1)S(1)}, u32[]{:S(2)}, u32[]{:S(2)}) collective-permute-start(bf16[32,1024]{1,0:T(8,128)(2,1)S(1)} %get-tuple-element.18), channel_id=1, source_target_pairs={{0,6},{2,4},{4,2},{6,0},{8,14},{10,12},{12,10},{14,8},{1,7},{3,5},... | collective-permute-start | bytes 196616 | tf_op jit(solution)/shard_map/ppermute | solution.py:30
  32.4 5.5 %collective-permute-start.16 = (bf16[32,1024]{1,0:T(8,128)(2,1)S(1)}, bf16[32,1024]{1,0:T(8,128)(2,1)S(1)}, u32[]{:S(2)}, u32[]{:S(2)}) collective-permute-start(bf16[32,1024]{1,0:T(8,128)(2,1)S(1)} %get-tuple-element.19), channel_id=1, source_target_pairs={{0,2},{2,0},{4,6},{6,4},{8,10},{10,8},{12,14},{14,12},{1,3},{3,1},... | collective-permute-start | bytes 196616 | tf_op jit(solution)/shard_map/ppermute | solution.py:30
  33.5 4.9 %collective-permute-start.15 = (bf16[32,1024]{1,0:T(8,128)(2,1)S(1)}, bf16[32,1024]{1,0:T(8,128)(2,1)S(1)}, u32[]{:S(2)}, u32[]{:S(2)}) collective-permute-start(bf16[32,1024]{1,0:T(8,128)(2,1)S(1)} %get-tuple-element.20), channel_id=1, source_target_pairs={{0,4},{2,6},{4,0},{6,2},{8,12},{10,14},{12,8},{14,10},{1,5},{3,7},... | collective-permute-start | bytes 196616 | tf_op jit(solution)/shard_map/ppermute | solution.py:30
  34.3 6.5 %collective-permute-start.5 = (bf16[32,1024]{1,0:T(8,128)(2,1)S(1)}, bf16[32,1024]{1,0:T(8,128)(2,1)S(1)}, u32[]{:S(2)}, u32[]{:S(2)}) collective-permute-start(bf16[32,1024]{1,0:T(8,128)(2,1)S(1)} %get-tuple-element.15), channel_id=1, source_target_pairs={{0,6},{2,4},{4,2},{6,0},{8,14},{10,12},{12,10},{14,8},{1,7},{3,5},... | collective-permute-start | bytes 196616 | tf_op jit(solution)/shard_map/ppermute | solution.py:30
  35.9 4.9 %collective-permute-start.7 = (bf16[32,1024]{1,0:T(8,128)(2,1)S(1)}, bf16[32,1024]{1,0:T(8,128)(2,1)S(1)}, u32[]{:S(2)}, u32[]{:S(2)}) collective-permute-start(bf16[32,1024]{1,0:T(8,128)(2,1)S(1)} %get-tuple-element.16), channel_id=1, source_target_pairs={{0,2},{2,0},{4,6},{6,4},{8,10},{10,8},{12,14},{14,12},{1,3},{3,1},... | collective-permute-start | bytes 196616 | tf_op jit(solution)/shard_map/ppermute | solution.py:30
  37.1 4.9 %collective-permute-start.6 = (bf16[32,1024]{1,0:T(8,128)(2,1)S(1)}, bf16[32,1024]{1,0:T(8,128)(2,1)S(1)}, u32[]{:S(2)}, u32[]{:S(2)}) collective-permute-start(bf16[32,1024]{1,0:T(8,128)(2,1)S(1)} %get-tuple-element.17), channel_id=1, source_target_pairs={{0,4},{2,6},{4,0},{6,2},{8,12},{10,14},{12,8},{14,10},{1,5},{3,7},... | collective-permute-start | bytes 196616 | tf_op jit(solution)/shard_map/ppermute | solution.py:30
  38.5 5.9 %collective-permute-start.17 = (bf16[32,1024]{1,0:T(8,128)(2,1)S(1)}, bf16[32,1024]{1,0:T(8,128)(2,1)S(1)}, u32[]{:S(2)}, u32[]{:S(2)}) collective-permute-start(bf16[32,1024]{1,0:T(8,128)(2,1)S(1)} %add_convert_fusion.2), channel_id=1, source_target_pairs={{0,8},{2,10},{4,12},{6,14},{8,0},{10,2},{12,4},{14,6},{1,9},{3,11}... | collective-permute-start | bytes 196616 | tf_op jit(solution)/shard_map/ppermute | solution.py:30

commit v2 on v1

--- a/solution.py
+++ b/solution.py
@@ -35,22 +35,25 @@
     near, far, place = pack(
         tokens, norm_gain, groups, picks, gates, rows, team, half, group_experts
     )
-    shifts = range(team - 1, 0, -1)
+    shifts = range(1, team)
+    column = jnp.arange(near.shape[1] - half, dtype=jnp.int32)[:, None]
+    expert = (ep % team) * local + jnp.arange(local, dtype=jnp.int32)[None, :]
+    pick_gates = ((column == expert) | (column == expert + group_experts)).astype(jnp.bfloat16)
 
-    def gates_of(piece):
-        pair = piece[:, half : half + 2 * group_experts].astype(jnp.float32)
-        return pair[:, :group_experts] + pair[:, group_experts:]
+    def gates_of(own):
+        return jnp.dot(own[:, half:], pick_gates, preferred_element_type=jnp.float32)
 
     got = across(far, mirror)
     last_got = lax.optimization_barrier(gates_of(got))
-    last_near = gates_of(near)
     near = [across(near, s) for s in shifts] + [near]
     got = [across(got, s) for s in shifts] + [got]
 
     def expert_rows(pieces, last):
         own = jnp.concatenate(pieces, axis=0)
-        weights = jnp.concatenate([gates_of(piece) for piece in pieces[:-1]] + [last], axis=0)
-        weights = lax.dynamic_slice_in_dim(weights, (ep % team) * local, local, 1)
+        if last is None:
+            weights = gates_of(own)
+        else:
+            weights = jnp.concatenate([gates_of(own[: -last.shape[0]]), last], axis=0)
         own = own[:, :half]
         other = swap(own)
         x = jnp.concatenate(
@@ -73,23 +76,23 @@
         send = jnp.where(tp == 0, high, low).astype(jnp.bfloat16)
         return (keep + swap(send).astype(jnp.float32)).astype(jnp.bfloat16)
 
-    def collect(part):
+    def collect(part, own):
         pieces = [part[i * rows : (i + 1) * rows] for i in range(team)]
-        total = pieces[-1].astype(jnp.float32)
-        for piece, s in zip(pieces, shifts):
-            total = total + across(piece, s).astype(jnp.float32)
+        sent = [across(piece, s) for piece, s in zip(pieces, shifts)]
+        total = sum(piece.astype(jnp.float32) for piece in (sent + pieces[-1:] if own else sent))
         return total.astype(jnp.bfloat16)
 
-    near_part = run_experts(*expert_rows(near, last_near))
+    def in_order(part, at):
+        return lax.dot_general(
+            place[at], part, (((0,), (0,)), ((), ())), preferred_element_type=jnp.float32
+        )
+
+    near_part = run_experts(*expert_rows(near, None))
     got_part = run_experts(*expert_rows(got, last_got))
-    far = across(collect(got_part), mirror)
-    near = collect(near_part)
-    out = lax.dot_general(
-        place,
-        jnp.concatenate([near, far], axis=0),
-        (((0,), (0,)), ((), ())),
-        preferred_element_type=jnp.float32,
-    )
+    far = across(collect(got_part, True), mirror)
+    near = collect(near_part, False)
+    own = lax.optimization_barrier(in_order(near_part[-rows:], slice(0, rows)))
+    out = own + in_order(jnp.concatenate([near, far], axis=0), slice(None))
     return out.astype(jnp.bfloat16)
 
 

time: 45.5 us -> 42.1 us (0.925)
  other arithmetic: 2.84 us -> 0.55 us
  waiting for transfers between devices: 11.4 us -> 9.49 us
  local copies, waits for them, and re-layouts: 0.88 us -> 1.95 us
  matrix products: 5.64 us -> 5.02 us
    ppermute x14, waiting for transfers between devices: 10.3 us -> 8.29 us  [across(): return lax.ppermute(x, 'ep', [(i, i ^ shift) for i in range(senders)])]
    dot_general x4, matrix products: 2.62 us -> 1.27 us  [run_experts(): g = jnp.dot(x, w_gate[j], preferred_element_type=jnp.float32)]
    concatenate x0 -> x1, local copies, waits for them, and re-layouts: none -> 0.9 us  [expert_rows(): own = jnp.concatenate(pieces, axis=0)]
    concatenate x2 -> x1, other arithmetic: 0.9 us -> 0.02 us  [expert_rows(): own = jnp.concatenate(pieces, axis=0)]
    dot_general x1 -> x5, matrix products: 0.86 us -> 1.59 us  [the longest x2 1.07 us: in_order(): lax.dot_general(place[at], part, (((0,), (0,)), ((), ())), preferred_elem...]
    convert_element_type x8 -> x0, other arithmetic: 0.72 us -> none  [gates_of(): pair = piece[:, half:half + 2 * group_experts].astype(jnp.float32)]
    unnamed x8 -> x11, local copies, waits for them, and re-layouts: 0.31 us -> 0.99 us
    add x8 -> x1, other arithmetic: 0.62 us -> 0.01 us  [on_device(): expert = ep % team * local + jnp.arange(local, dtype=jnp.int32)[None, :]]
  transfers between devices with their start and end apart: 18 -> 18, of which waited for: 8 -> 8; matrix products, arithmetic and copies ran while one was open for 16% -> 13% of each run, Pallas kernels for 0% -> 0%
where the time goes in v2:
time: 42.1 us; the launch traced here: 41.9 us
  starting transfers between devices  22.5 us (53%)
  waiting for transfers between devices  9.49 us (23%)
  matrix products  5.02 us (12%)
  Pallas kernels  2.12 us (5%)
  local copies, waits for them, and re-layouts  1.95 us (5%)
  other arithmetic  0.55 us (1%)
    ppermute x14, starting transfers between devices, across(): return lax.ppermute(x, 'ep', [(i, i ^ shift) for i in range(senders)])  21.7 us
    ppermute x14, waiting for transfers between devices, across(): return lax.ppermute(x, 'ep', [(i, i ^ shift) for i in range(senders)])  8.29 us
    pallas_call x1, Pallas kernels, pack(): pl.pallas_call(kernel, out_shape=(block, block, jax.ShapeDtypeStruct((GRO...  2.12 us
    dot_general x4, matrix products, run_experts(): u = jnp.dot(x, w_up[j], preferred_element_type=jnp.float32)  1.28 us
    dot_general x4, matrix products, run_experts(): g = jnp.dot(x, w_gate[j], preferred_element_type=jnp.float32)  1.27 us
    ppermute x4, waiting for transfers between devices, swap(): return lax.ppermute(x, 'tp', [(i, cores - 1 - i) for i in range(cores)])  1.2 us
    dot_general x2, matrix products, in_order(): lax.dot_general(place[at], part, (((0,), (0,)), ((), ())), preferred_elem...  1.07 us
    unnamed x11, local copies, waits for them, and re-layouts  0.99 us
  transfers between devices with their start and end apart: 18, of which 8 were waited for; matrix products, arithmetic and copies ran while one was open for 13% of the time, Pallas kernels for 0%

profile of v2, /device:TPU:0, one launch (start us, length us, event | category | flops | bytes accessed | tf_op | source)
XLA Modules:
  0.0 41.9 jit_solution(3638907174576334592)
XLA Ops:
  0.0 0.0 copy-start
  0.0 2.1 %shard_map.82 = (bf16[32,1152]{1,0:T(8,128)(2,1)}, bf16[32,1152]{1,0:T(8,128)(2,1)}, bf16[64,64]{1,0:T(8,128)(2,1)}) custom-call(bf16[64,2048]{1,0:T(8,128)(2,1)} %tok_ref.1, f32[1,2048]{1,0:T(1,128)} %bitcast.46, s32[1,64]{1,0:T(1,128)} %bitcast.49, s32[4,64]{1,0:T(4,128)} %bitcast.47, f32[4,64]{1,0:T(4,128)} %bitcast.48), custom_call_target="tpu_custom_call" | custom-call | tf_op jit(solution)/shard_map/pallas_call | solution.py:139
  2.1 4.0 %collective-permute-start.2 = (bf16[32,1152]{1,0:T(8,128)(2,1)}, bf16[32,1152]{1,0:T(8,128)(2,1)S(1)}, u32[]{:S(2)}, u32[]{:S(2)}) collective-permute-start(bf16[32,1152]{1,0:T(8,128)(2,1)} %get-tuple-element.9), channel_id=1, source_target_pairs={{0,6},{2,4},{4,2},{6,0},{8,14},{10,12},{12,10},{14,8},{1,7},{3,5},... | collective-permute-start | bytes 221192 | tf_op jit(solution)/shard_map/ppermute | solution.py:30
  6.1 0.4 %collective-permute-start.1 = (bf16[32,1152]{1,0:T(8,128)(2,1)}, bf16[32,1152]{1,0:T(8,128)(2,1)S(1)}, u32[]{:S(2)}, u32[]{:S(2)}) collective-permute-start(bf16[32,1152]{1,0:T(8,128)(2,1)} %get-tuple-element.9), channel_id=1, source_target_pairs={{0,4},{2,6},{4,0},{6,2},{8,12},{10,14},{12,8},{14,10},{1,5},{3,7},... | collective-permute-start | bytes 221192 | tf_op jit(solution)/shard_map/ppermute | solution.py:30
  6.6 0.1 collective-permute-start
  6.7 3.0 %collective-permute-start.8 = (bf16[32,1152]{1,0:T(8,128)(2,1)}, bf16[32,1152]{1,0:T(8,128)(2,1)S(1)}, u32[]{:S(2)}, u32[]{:S(2)}) collective-permute-start(bf16[32,1152]{1,0:T(8,128)(2,1)} %get-tuple-element.10), channel_id=1, source_target_pairs={{0,8},{2,10},{4,12},{6,14},{8,0},{10,2},{12,4},{14,6},{1,9},{3,11}... | collective-permute-start | bytes 221192 | tf_op jit(solution)/shard_map/ppermute | solution.py:30
  9.7 1.5 %collective-permute-done = bf16[32,1152]{1,0:T(8,128)(2,1)S(1)} collective-permute-done((bf16[32,1152]{1,0:T(8,128)(2,1)}, bf16[32,1152]{1,0:T(8,128)(2,1)S(1)}, u32[]{:S(2)}, u32[]{:S(2)}) %collective-permute-start) | collective-permute-done | bytes 73760 | tf_op jit(solution)/shard_map/ppermute | solution.py:30
  11.2 0.3 collective-permute-done.1
  11.5 0.0 collective-permute-done.2
  11.5 0.9 %constant_dynamic-update-slice_fusion = bf16[128,1152]{1,0:T(8,128)(2,1)S(1)} fusion(bf16[128,1152]{1,0:T(8,128)(2,1)S(1)} %constant_dynamic-update-slice_fusion.1, bf16[32,1152]{1,0:T(8,128)(2,1)} %get-tuple-element.9), kind=kLoop, calls=%fused_computation.74 | loop fusion | bytes 147456 | tf_op jit(solution)/shard_map/concatenate | solution.py:52
  12.4 0.2 fusion.43
  12.6 0.0 collective-permute-done.8
  12.6 0.2 fusion.39
  12.8 2.6 %collective-permute-start.11 = (bf16[32,1152]{1,0:T(8,128)(2,1)S(1)}, bf16[32,1152]{1,0:T(8,128)(2,1)S(1)}, u32[]{:S(2)}, u32[]{:S(2)}) collective-permute-start(bf16[32,1152]{1,0:T(8,128)(2,1)S(1)} %collective-permute-done.8), channel_id=1, source_target_pairs={{0,6},{2,4},{4,2},{6,0},{8,14},{10,12},{12,10},{14,8},{1,7},{3,5},... | collective-permute-start | bytes 221192 | tf_op jit(solution)/shard_map/ppermute | solution.py:30
  15.4 1.5 %collective-permute-start.10 = (bf16[32,1152]{1,0:T(8,128)(2,1)S(1)}, bf16[32,1152]{1,0:T(8,128)(2,1)S(1)}, u32[]{:S(2)}, u32[]{:S(2)}) collective-permute-start(bf16[32,1152]{1,0:T(8,128)(2,1)S(1)} %collective-permute-done.8), channel_id=1, source_target_pairs={{0,4},{2,6},{4,0},{6,2},{8,12},{10,14},{12,8},{14,10},{1,5},{3,7},... | collective-permute-start | bytes 221192 | tf_op jit(solution)/shard_map/ppermute | solution.py:30
  16.9 0.0 collective-permute-start.9
  16.9 0.1 collective-permute-start.3
  17.0 1.8 %collective-permute-done.11 = bf16[32,1152]{1,0:T(8,128)(2,1)S(1)} collective-permute-done((bf16[32,1152]{1,0:T(8,128)(2,1)S(1)}, bf16[32,1152]{1,0:T(8,128)(2,1)S(1)}, u32[]{:S(2)}, u32[]{:S(2)}) %collective-permute-start.11) | collective-permute-done | bytes 73760 | tf_op jit(solution)/shard_map/ppermute | solution.py:30
  18.8 1.2 %collective-permute-done.10 = bf16[32,1152]{1,0:T(8,128)(2,1)S(1)} collective-permute-done((bf16[32,1152]{1,0:T(8,128)(2,1)S(1)}, bf16[32,1152]{1,0:T(8,128)(2,1)S(1)}, u32[]{:S(2)}, u32[]{:S(2)}) %collective-permute-start.10) | collective-permute-done | bytes 73760 | tf_op jit(solution)/shard_map/ppermute | solution.py:30
  20.0 1.2 %collective-permute-done.9 = bf16[32,1152]{1,0:T(8,128)(2,1)S(1)} collective-permute-done((bf16[32,1152]{1,0:T(8,128)(2,1)S(1)}, bf16[32,1152]{1,0:T(8,128)(2,1)S(1)}, u32[]{:S(2)}, u32[]{:S(2)}) %collective-permute-start.9) | collective-permute-done | bytes 73760 | tf_op jit(solution)/shard_map/ppermute | solution.py:30
  21.3 0.1 collective-permute-start.12
  21.3 0.2 fusion.41
  21.5 0.1 pad_maximum_fusion.9
  21.6 0.0 collective-permute-done.3
  21.6 0.1 broadcast_select_fusion.3
  21.7 0.0 copy-start.3
  21.7 0.3 fusion.7
  22.0 0.3 fusion.15
  22.3 0.9 %copy-done.3 = bf16[2,2048,256]{2,1,0:T(8,128)(2,1)S(1)} copy-done((bf16[2,2048,256]{2,1,0:T(8,128)(2,1)S(1)}, bf16[2,2048,256]{2,1,0:T(8,128)(2,1)}, u32[]{:S(2)}) %copy-start.3) | copy-done | bytes 2097176
  23.3 0.3 multiply_convert_fusion.2
  23.6 0.3 multiply_convert_fusion.3
  23.9 0.0 copy-done
  23.9 0.4 %fusion.25 = f32[128,2048]{1,0:T(8,128)S(1)} fusion(bf16[512,2048]{1,0:T(8,128)(2,1)S(1)} %bitcast.44, bf16[128,256]{1,0:T(8,128)(2,1)S(1)} %multiply_convert_fusion.2, bf16[128,256]{1,0:T(8,128)(2,1)S(1)} %multiply_convert_fusion.3), kind=kOutput, calls=%fused_computation.39 | convolution fusion | flops 268697600 | bytes 3276800 | tf_op jit(solution)/shard_map/dot_general | solution.py:71
  24.4 0.1 select_convert_fusion.1
  24.4 0.6 %collective-permute-start.4 = (bf16[128,1024]{1,0:T(8,128)(2,1)S(1)}, bf16[128,1024]{1,0:T(8,128)(2,1)S(1)}, u32[]{:S(2)}, u32[]{:S(2)}) collective-permute-start(bf16[128,1024]{1,0:T(8,128)(2,1)S(1)} %select_convert_fusion.1), channel_id=1, source_target_pairs={{0,1},{1,0},{2,3},{3,2},{4,5},{5,4},{6,7},{7,6},{8,9},{9,8},{10,11... | collective-permute-start | bytes 786440 | tf_op jit(solution)/shard_map/ppermute | solution.py:33
  25.0 0.0 collective-permute-done.12
  25.1 0.3 fusion.5
  25.4 0.3 fusion.13
  25.7 0.3 multiply_convert_fusion
  26.0 0.3 multiply_convert_fusion.1
  26.4 0.4 %fusion.29 = f32[128,2048]{1,0:T(8,128)S(1)} fusion(bf16[512,2048]{1,0:T(8,128)(2,1)S(1)} %bitcast.45, bf16[128,256]{1,0:T(8,128)(2,1)S(1)} %multiply_convert_fusion, bf16[128,256]{1,0:T(8,128)(2,1)S(1)} %multiply_convert_fusion.1), kind=kOutput, calls=%fused_computation.43 | convolution fusion | flops 268697600 | bytes 3276800 | tf_op jit(solution)/shard_map/dot_general | solution.py:71
  26.8 0.1 select_convert_fusion
  26.9 0.1 collective-permute-start.13
  27.0 0.0 collective-permute-done.4
  27.0 0.1 add_convert_fusion.1
  27.1 0.0 copy-done.1
  27.1 0.2 fusion.36
  27.3 1.2 %collective-permute-done.13 = bf16[128,1024]{1,0:T(8,128)(2,1)S(1)} collective-permute-done((bf16[128,1024]{1,0:T(8,128)(2,1)S(1)}, bf16[128,1024]{1,0:T(8,128)(2,1)S(1)}, u32[]{:S(2)}, u32[]{:S(2)}) %collective-permute-start.13) | collective-permute-done | bytes 262176 | tf_op jit(solution)/shard_map/ppermute | solution.py:33
  28.5 0.1 add_convert_fusion
  28.6 0.3 collective-permute-start.14
  28.9 1.7 %collective-permute-start.16 = (bf16[32,1024]{1,0:T(8,128)(2,1)S(1)}, bf16[32,1024]{1,0:T(8,128)(2,1)S(1)}, u32[]{:S(2)}, u32[]{:S(2)}) collective-permute-start(bf16[32,1024]{1,0:T(8,128)(2,1)S(1)} %get-tuple-element.19), channel_id=1, source_target_pairs={{0,6},{2,4},{4,2},{6,0},{8,14},{10,12},{12,10},{14,8},{1,7},{3,5},... | collective-permute-start | bytes 196616 | tf_op jit(solution)/shard_map/ppermute | solution.py:30
  30.6 1.5 %collective-permute-start.15 = (bf16[32,1024]{1,0:T(8,128)(2,1)S(1)}, bf16[32,1024]{1,0:T(8,128)(2,1)S(1)}, u32[]{:S(2)}, u32[]{:S(2)}) collective-permute-start(bf16[32,1024]{1,0:T(8,128)(2,1)S(1)} %get-tuple-element.20), channel_id=1, source_target_pairs={{0,4},{2,6},{4,0},{6,2},{8,12},{10,14},{12,8},{14,10},{1,5},{3,7},... | collective-permute-start | bytes 196616 | tf_op jit(solution)/shard_map/ppermute | solution.py:30
  32.2 0.3 collective-permute-start.5
  32.5 1.7 %collective-permute-start.7 = (bf16[32,1024]{1,0:T(8,128)(2,1)S(1)}, bf16[32,1024]{1,0:T(8,128)(2,1)S(1)}, u32[]{:S(2)}, u32[]{:S(2)}) collective-permute-start(bf16[32,1024]{1,0:T(8,128)(2,1)S(1)} %get-tuple-element.16), channel_id=1, source_target_pairs={{0,6},{2,4},{4,2},{6,0},{8,14},{10,12},{12,10},{14,8},{1,7},{3,5},... | collective-permute-start | bytes 196616 | tf_op jit(solution)/shard_map/ppermute | solution.py:30
  34.2 0.0 collective-permute-done.14
  34.2 1.5 %collective-permute-start.6 = (bf16[32,1024]{1,0:T(8,128)(2,1)S(1)}, bf16[32,1024]{1,0:T(8,128)(2,1)S(1)}, u32[]{:S(2)}, u32[]{:S(2)}) collective-permute-start(bf16[32,1024]{1,0:T(8,128)(2,1)S(1)} %get-tuple-element.17), channel_id=1, source_target_pairs={{0,4},{2,6},{4,0},{6,2},{8,12},{10,14},{12,8},{14,10},{1,5},{3,7},... | collective-permute-start | bytes 196616 | tf_op jit(solution)/shard_map/ppermute | solution.py:30
  35.7 0.0 collective-permute-done.16
  35.7 0.0 collective-permute-done.15
  35.8 3.0 %collective-permute-start.17 = (bf16[32,1024]{1,0:T(8,128)(2,1)S(1)}, bf16[32,1024]{1,0:T(8,128)(2,1)S(1)}, u32[]{:S(2)}, u32[]{:S(2)}) collective-permute-start(bf16[32,1024]{1,0:T(8,128)(2,1)S(1)} %add_convert_fusion.2), channel_id=1, source_target_pairs={{0,8},{2,10},{4,12},{6,14},{8,0},{10,2},{12,4},{14,6},{1,9},{3,11}... | collective-permute-start | bytes 196616 | tf_op jit(solution)/shard_map/ppermute | solution.py:30
  38.7 0.0 collective-permute-done.5
  38.8 0.0 collective-permute-done.7
  38.8 0.6 %collective-permute-done.6 = bf16[32,1024]{1,0:T(8,128)(2,1)S(1)} collective-permute-done((bf16[32,1024]{1,0:T(8,128)(2,1)S(1)}, bf16[32,1024]{1,0:T(8,128)(2,1)S(1)}, u32[]{:S(2)}, u32[]{:S(2)}) %collective-permute-start.6) | collective-permute-done | bytes 65568 | tf_op jit(solution)/shard_map/ppermute | solution.py:30
  39.4 1.6 %collective-permute-done.17 = bf16[32,1024]{1,0:T(8,128)(2,1)S(1)} collective-permute-done((bf16[32,1024]{1,0:T(8,128)(2,1)S(1)}, bf16[32,1024]{1,0:T(8,128)(2,1)S(1)}, u32[]{:S(2)}, u32[]{:S(2)}) %collective-permute-start.17) | collective-permute-done | bytes 65568 | tf_op jit(solution)/shard_map/ppermute | solution.py:30
  41.0 0.9 %fusion = bf16[64,1024]{1,0:T(8,128)(2,1)} fusion(f32[64,1024]{1,0:T(8,128)S(1)} %fusion.36, bf16[64,64]{1,0:T(8,128)(2,1)S(1)} %copy-done.1, bf16[32,1024]{1,0:T(8,128)(2,1)S(1)} %collective-permute-done.17, bf16[32,1024]{1,0:T(8,128)(2,1)S(1)} %add_convert_fusion.3), kind=kOutput, calls=%fused_computation.1 | convolution fusion | flops 8781824 | bytes 532480 | tf_op jit(solution)/shard_map/dot_general | solution.py:86
  (16 shorter events, 0.2 us)
Async XLA Ops:
  0.0 23.9 %copy-start = (bf16[2,256,2048]{2,1,0:T(8,128)(2,1)S(1)}, bf16[2,256,2048]{2,1,0:T(8,128)(2,1)}, u32[]{:S(2)}) copy-start(bf16[2,256,2048]{2,1,0:T(8,128)(2,1)} %param.15) | copy-start | bytes 6291460
  2.1 9.4 %collective-permute-start.2 = (bf16[32,1152]{1,0:T(8,128)(2,1)}, bf16[32,1152]{1,0:T(8,128)(2,1)S(1)}, u32[]{:S(2)}, u32[]{:S(2)}) collective-permute-start(bf16[32,1152]{1,0:T(8,128)(2,1)} %get-tuple-element.9), channel_id=1, source_target_pairs={{0,6},{2,4},{4,2},{6,0},{8,14},{10,12},{12,10},{14,8},{1,7},{3,5},... | collective-permute-start | bytes 221192 | tf_op jit(solution)/shard_map/ppermute | solution.py:30
  6.1 5.4 %collective-permute-start.1 = (bf16[32,1152]{1,0:T(8,128)(2,1)}, bf16[32,1152]{1,0:T(8,128)(2,1)S(1)}, u32[]{:S(2)}, u32[]{:S(2)}) collective-permute-start(bf16[32,1152]{1,0:T(8,128)(2,1)} %get-tuple-element.9), channel_id=1, source_target_pairs={{0,4},{2,6},{4,0},{6,2},{8,12},{10,14},{12,8},{14,10},{1,5},{3,7},... | collective-permute-start | bytes 221192 | tf_op jit(solution)/shard_map/ppermute | solution.py:30
  6.6 4.6 %collective-permute-start = (bf16[32,1152]{1,0:T(8,128)(2,1)}, bf16[32,1152]{1,0:T(8,128)(2,1)S(1)}, u32[]{:S(2)}, u32[]{:S(2)}) collective-permute-start(bf16[32,1152]{1,0:T(8,128)(2,1)} %get-tuple-element.9), channel_id=1, source_target_pairs={{0,2},{2,0},{4,6},{6,4},{8,10},{10,8},{12,14},{14,12},{1,3},{3,1},... | collective-permute-start | bytes 221192 | tf_op jit(solution)/shard_map/ppermute | solution.py:30
  6.7 5.9 %collective-permute-start.8 = (bf16[32,1152]{1,0:T(8,128)(2,1)}, bf16[32,1152]{1,0:T(8,128)(2,1)S(1)}, u32[]{:S(2)}, u32[]{:S(2)}) collective-permute-start(bf16[32,1152]{1,0:T(8,128)(2,1)} %get-tuple-element.10), channel_id=1, source_target_pairs={{0,8},{2,10},{4,12},{6,14},{8,0},{10,2},{12,4},{14,6},{1,9},{3,11}... | collective-permute-start | bytes 221192 | tf_op jit(solution)/shard_map/ppermute | solution.py:30
  9.7 12.0 %copy-start.2 = (bf16[2,2048,256]{2,1,0:T(8,128)(2,1)S(1)}, bf16[2,2048,256]{2,1,0:T(8,128)(2,1)}, u32[]{:S(2)}) copy-start(bf16[2,2048,256]{2,1,0:T(8,128)(2,1)} %param.13) | copy-start | bytes 6291460
  12.8 6.0 %collective-permute-start.11 = (bf16[32,1152]{1,0:T(8,128)(2,1)S(1)}, bf16[32,1152]{1,0:T(8,128)(2,1)S(1)}, u32[]{:S(2)}, u32[]{:S(2)}) collective-permute-start(bf16[32,1152]{1,0:T(8,128)(2,1)S(1)} %collective-permute-done.8), channel_id=1, source_target_pairs={{0,6},{2,4},{4,2},{6,0},{8,14},{10,12},{12,10},{14,8},{1,7},{3,5},... | collective-permute-start | bytes 221192 | tf_op jit(solution)/shard_map/ppermute | solution.py:30
  15.4 4.6 %collective-permute-start.10 = (bf16[32,1152]{1,0:T(8,128)(2,1)S(1)}, bf16[32,1152]{1,0:T(8,128)(2,1)S(1)}, u32[]{:S(2)}, u32[]{:S(2)}) collective-permute-start(bf16[32,1152]{1,0:T(8,128)(2,1)S(1)} %collective-permute-done.8), channel_id=1, source_target_pairs={{0,4},{2,6},{4,0},{6,2},{8,12},{10,14},{12,8},{14,10},{1,5},{3,7},... | collective-permute-start | bytes 221192 | tf_op jit(solution)/shard_map/ppermute | solution.py:30
  16.9 4.4 %collective-permute-start.9 = (bf16[32,1152]{1,0:T(8,128)(2,1)S(1)}, bf16[32,1152]{1,0:T(8,128)(2,1)S(1)}, u32[]{:S(2)}, u32[]{:S(2)}) collective-permute-start(bf16[32,1152]{1,0:T(8,128)(2,1)S(1)} %collective-permute-done.8), channel_id=1, source_target_pairs={{0,2},{2,0},{4,6},{6,4},{8,10},{10,8},{12,14},{14,12},{1,3},{3,1},... | collective-permute-start | bytes 221192 | tf_op jit(solution)/shard_map/ppermute | solution.py:30
  16.9 4.7 %collective-permute-start.3 = (bf16[128,1024]{1,0:T(8,128)(2,1)S(1)}, bf16[128,1024]{1,0:T(8,128)(2,1)S(1)}, u32[]{:S(2)}, u32[]{:S(2)}) collective-permute-start(bf16[128,1024]{1,0:T(8,128)(2,1)S(1)} %slice.111), channel_id=1, source_target_pairs={{0,1},{1,0},{2,3},{3,2},{4,5},{5,4},{6,7},{7,6},{8,9},{9,8},{10,11... | collective-permute-start | bytes 786440 | tf_op jit(solution)/shard_map/ppermute | solution.py:33
  21.3 3.8 %collective-permute-start.12 = (bf16[128,1024]{1,0:T(8,128)(2,1)S(1)}, bf16[128,1024]{1,0:T(8,128)(2,1)S(1)}, u32[]{:S(2)}, u32[]{:S(2)}) collective-permute-start(bf16[128,1024]{1,0:T(8,128)(2,1)S(1)} %pad_maximum_fusion.2), channel_id=1, source_target_pairs={{0,1},{1,0},{2,3},{3,2},{4,5},{5,4},{6,7},{7,6},{8,9},{9,8},{10,11... | collective-permute-start | bytes 786440 | tf_op jit(solution)/shard_map/ppermute | solution.py:33
  21.7 1.6 %copy-start.3 = (bf16[2,2048,256]{2,1,0:T(8,128)(2,1)S(1)}, bf16[2,2048,256]{2,1,0:T(8,128)(2,1)}, u32[]{:S(2)}) copy-start(bf16[2,2048,256]{2,1,0:T(8,128)(2,1)} %param.14) | copy-start | bytes 6291460
  24.4 2.5 %collective-permute-start.4 = (bf16[128,1024]{1,0:T(8,128)(2,1)S(1)}, bf16[128,1024]{1,0:T(8,128)(2,1)S(1)}, u32[]{:S(2)}, u32[]{:S(2)}) collective-permute-start(bf16[128,1024]{1,0:T(8,128)(2,1)S(1)} %select_convert_fusion.1), channel_id=1, source_target_pairs={{0,1},{1,0},{2,3},{3,2},{4,5},{5,4},{6,7},{7,6},{8,9},{9,8},{10,11... | collective-permute-start | bytes 786440 | tf_op jit(solution)/shard_map/ppermute | solution.py:33
  26.4 0.7 %copy-start.1 = (bf16[64,64]{1,0:T(8,128)(2,1)S(1)}, bf16[64,64]{1,0:T(8,128)(2,1)}, u32[]{:S(2)}) copy-start(bf16[64,64]{1,0:T(8,128)(2,1)} %get-tuple-element.8) | copy-start | bytes 24580
  26.9 1.6 %collective-permute-start.13 = (bf16[128,1024]{1,0:T(8,128)(2,1)S(1)}, bf16[128,1024]{1,0:T(8,128)(2,1)S(1)}, u32[]{:S(2)}, u32[]{:S(2)}) collective-permute-start(bf16[128,1024]{1,0:T(8,128)(2,1)S(1)} %select_convert_fusion), channel_id=1, source_target_pairs={{0,1},{1,0},{2,3},{3,2},{4,5},{5,4},{6,7},{7,6},{8,9},{9,8},{10,11... | collective-permute-start | bytes 786440 | tf_op jit(solution)/shard_map/ppermute | solution.py:33
  28.6 5.6 %collective-permute-start.14 = (bf16[32,1024]{1,0:T(8,128)(2,1)S(1)}, bf16[32,1024]{1,0:T(8,128)(2,1)S(1)}, u32[]{:S(2)}, u32[]{:S(2)}) collective-permute-start(bf16[32,1024]{1,0:T(8,128)(2,1)S(1)} %get-tuple-element.18), channel_id=1, source_target_pairs={{0,2},{2,0},{4,6},{6,4},{8,10},{10,8},{12,14},{14,12},{1,3},{3,1},... | collective-permute-start | bytes 196616 | tf_op jit(solution)/shard_map/ppermute | solution.py:30
  28.9 6.8 %collective-permute-start.16 = (bf16[32,1024]{1,0:T(8,128)(2,1)S(1)}, bf16[32,1024]{1,0:T(8,128)(2,1)S(1)}, u32[]{:S(2)}, u32[]{:S(2)}) collective-permute-start(bf16[32,1024]{1,0:T(8,128)(2,1)S(1)} %get-tuple-element.19), channel_id=1, source_target_pairs={{0,6},{2,4},{4,2},{6,0},{8,14},{10,12},{12,10},{14,8},{1,7},{3,5},... | collective-permute-start | bytes 196616 | tf_op jit(solution)/shard_map/ppermute | solution.py:30
  30.6 5.1 %collective-permute-start.15 = (bf16[32,1024]{1,0:T(8,128)(2,1)S(1)}, bf16[32,1024]{1,0:T(8,128)(2,1)S(1)}, u32[]{:S(2)}, u32[]{:S(2)}) collective-permute-start(bf16[32,1024]{1,0:T(8,128)(2,1)S(1)} %get-tuple-element.20), channel_id=1, source_target_pairs={{0,4},{2,6},{4,0},{6,2},{8,12},{10,14},{12,8},{14,10},{1,5},{3,7},... | collective-permute-start | bytes 196616 | tf_op jit(solution)/shard_map/ppermute | solution.py:30
  32.2 6.6 %collective-permute-start.5 = (bf16[32,1024]{1,0:T(8,128)(2,1)S(1)}, bf16[32,1024]{1,0:T(8,128)(2,1)S(1)}, u32[]{:S(2)}, u32[]{:S(2)}) collective-permute-start(bf16[32,1024]{1,0:T(8,128)(2,1)S(1)} %get-tuple-element.15), channel_id=1, source_target_pairs={{0,2},{2,0},{4,6},{6,4},{8,10},{10,8},{12,14},{14,12},{1,3},{3,1},... | collective-permute-start | bytes 196616 | tf_op jit(solution)/shard_map/ppermute | solution.py:30
  32.5 6.3 %collective-permute-start.7 = (bf16[32,1024]{1,0:T(8,128)(2,1)S(1)}, bf16[32,1024]{1,0:T(8,128)(2,1)S(1)}, u32[]{:S(2)}, u32[]{:S(2)}) collective-permute-start(bf16[32,1024]{1,0:T(8,128)(2,1)S(1)} %get-tuple-element.16), channel_id=1, source_target_pairs={{0,6},{2,4},{4,2},{6,0},{8,14},{10,12},{12,10},{14,8},{1,7},{3,5},... | collective-permute-start | bytes 196616 | tf_op jit(solution)/shard_map/ppermute | solution.py:30
  34.2 5.2 %collective-permute-start.6 = (bf16[32,1024]{1,0:T(8,128)(2,1)S(1)}, bf16[32,1024]{1,0:T(8,128)(2,1)S(1)}, u32[]{:S(2)}, u32[]{:S(2)}) collective-permute-start(bf16[32,1024]{1,0:T(8,128)(2,1)S(1)} %get-tuple-element.17), channel_id=1, source_target_pairs={{0,4},{2,6},{4,0},{6,2},{8,12},{10,14},{12,8},{14,10},{1,5},{3,7},... | collective-permute-start | bytes 196616 | tf_op jit(solution)/shard_map/ppermute | solution.py:30
  35.8 5.2 %collective-permute-start.17 = (bf16[32,1024]{1,0:T(8,128)(2,1)S(1)}, bf16[32,1024]{1,0:T(8,128)(2,1)S(1)}, u32[]{:S(2)}, u32[]{:S(2)}) collective-permute-start(bf16[32,1024]{1,0:T(8,128)(2,1)S(1)} %add_convert_fusion.2), channel_id=1, source_target_pairs={{0,8},{2,10},{4,12},{6,14},{8,0},{10,2},{12,4},{14,6},{1,9},{3,11}... | collective-permute-start | bytes 196616 | tf_op jit(solution)/shard_map/ppermute | solution.py:30
